TPU v7x, 32 devices: a whole 2x2x4 slice. The times are simulated.
32 devices in a mesh: ep: 8 (over z, y), tp: 4 (over x, core).
Axes of the slice: x: 2, y: 2, z: 4, core: 2. Of those that a mesh axis runs over, the one named last changes fastest.
Arguments:
- tokens: bfloat16 [1024, 2048], P('ep'), may hold values from -36 to 36, as said below
- norm_gain: float32 [2048], replicated, may hold values from 0.1 to 1.9
- chosen: int32 [8, 256], replicated, may hold values from 0 to 1023, as said below
- slot_weight: float32 [8, 256], replicated, may hold values from 0.1 to 1
- gate_weight: bfloat16 [8, 2048, 4096], P(None, 'ep', 'tp'), may hold values from -0.125 to 0.125
- up_weight: bfloat16 [8, 2048, 4096], P(None, 'ep', 'tp'), may hold values from -0.125 to 0.125
- down_weight: bfloat16 [8, 2048, 4096], P(None, 'ep', 'tp'), may hold values from -0.09375 to 0.09375
Outputs:
- mixed: bfloat16 [1024, 2048], P('ep', 'tp')
Inputs may be any that keep to these rules, and one draw needn't show every extreme that they name: `tokens`: each entry is the scaled entry of a bounded draw; rows and features differ in scale. `chosen`: the 256 slots of an expert name distinct tokens. Slots of an expert fall into aligned blocks of 256; within a block the token numbers ascend, and at most 64 of them lie among the 128 tokens of one index of ep (tokens i * 128 onward belong to index i); in every block some index supplies exactly 64.
All inputs are finite; a program needn't handle non-finite values.
Results may differ from a plain program's by a relative error of at most 0.019.
Values may be sent and summed in bfloat16 or wider, within the bound.
A program may use at most 64 MiB of HBM per device.

v0:
```python
import jax
import jax.numpy as jnp
from jax import lax
from jax.sharding import PartitionSpec as P

EPSILON = 1e-06


def body(tokens, norm_gain, chosen, slot_weight, gate_weight, up_weight, down_weight):
    expert_devices = lax.axis_size("ep")
    width_devices = lax.axis_size("tp")
    device_index = lax.axis_index("ep")
    width_index = lax.axis_index("tp")
    local_tokens = tokens.shape[0]
    model_width = tokens.shape[1]
    expert_total = chosen.shape[0]
    group_size = expert_devices // expert_total
    slots_piece = chosen.shape[1] // group_size
    seat_count = 4 * local_tokens // expert_devices
    buffer_rows = expert_devices * seat_count
    column_width = model_width // width_devices
    values = tokens.astype(jnp.float32)
    scaled = values * lax.rsqrt(jnp.mean(values * values, axis=1, keepdims=True) + EPSILON)
    normed = (scaled * norm_gain).astype(jnp.bfloat16)
    piece_tokens = chosen.reshape(expert_devices, slots_piece)
    piece_weights = slot_weight.reshape(expert_devices, slots_piece)
    owners = piece_tokens // local_tokens
    is_mine = owners == device_index
    earlier = jnp.sum((owners < device_index).astype(jnp.int32), axis=1, keepdims=True)
    seat_index = jnp.arange(slots_piece, dtype=jnp.int32)[None, :] - earlier
    local_index = piece_tokens - device_index * local_tokens
    seat_range = jnp.arange(seat_count, dtype=jnp.int32)
    matches = is_mine[:, None, :] & (seat_index[:, None, :] == seat_range[None, :, None])
    filled = jnp.any(matches, axis=2).reshape(buffer_rows)
    source_index = jnp.sum(jnp.where(matches, local_index[:, None, :], 0), axis=2).reshape(
        buffer_rows
    )
    seat_weight = jnp.sum(jnp.where(matches, piece_weights[:, None, :], 0.0), axis=2).reshape(
        buffer_rows
    )
    my_tokens = lax.dynamic_index_in_dim(piece_tokens, device_index, 0, keepdims=False)
    my_owners = my_tokens // local_tokens
    before = jnp.sum((my_owners[None, :] < my_owners[:, None]).astype(jnp.int32), axis=1)
    arrival_row = my_owners * seat_count + jnp.arange(slots_piece, dtype=jnp.int32) - before
    gate_send = jnp.repeat(gate_weight, group_size, axis=0)
    up_send = jnp.repeat(up_weight, group_size, axis=0)
    down_send = jnp.repeat(down_weight, group_size, axis=0)
    gate_full, up_full = (
        lax.all_to_all(gate_send, "ep", split_axis=0, concat_axis=1, tiled=True),
        lax.all_to_all(up_send, "ep", split_axis=0, concat_axis=1, tiled=True),
    )
    down_full = lax.all_to_all(down_send, "ep", split_axis=0, concat_axis=1, tiled=True)
    empty_value = jnp.zeros((), jnp.bfloat16)
    columns = lax.dynamic_slice_in_dim(normed, width_index * column_width, column_width, 1)
    outgoing = jnp.where(filled[:, None], jnp.take(columns, source_index, axis=0), empty_value)
    narrow = lax.all_to_all(
        outgoing.reshape(expert_devices, seat_count, column_width),
        "ep",
        split_axis=0,
        concat_axis=0,
        tiled=True,
    )
    arrived = lax.all_gather(narrow, "tp", axis=2, tiled=True)
    slot_rows = jnp.take(arrived.reshape(buffer_rows, model_width), arrival_row, axis=0)
    gate_part = jnp.dot(slot_rows, gate_full[0], preferred_element_type=jnp.float32)
    up_part = jnp.dot(slot_rows, up_full[0], preferred_element_type=jnp.float32)
    hidden = (jax.nn.silu(gate_part) * up_part).astype(jnp.bfloat16)
    down_rows = down_full[0]
    summed = lax.psum_scatter(
        jnp.einsum("df,bf->db", down_rows, hidden, preferred_element_type=jnp.float32).astype(
            jnp.bfloat16
        ),
        "tp",
        scatter_dimension=0,
        tiled=True,
    )
    buffer_range = jnp.arange(buffer_rows, dtype=jnp.int32)
    hits = arrival_row[None, :] == buffer_range[:, None]
    back_index = jnp.sum(
        jnp.where(hits, jnp.arange(slots_piece, dtype=jnp.int32)[None, :], 0), axis=1
    )
    expert_out = jnp.take(summed, back_index, axis=1).reshape(
        column_width, expert_devices, seat_count
    )
    returned = lax.all_to_all(expert_out, "ep", split_axis=1, concat_axis=1, tiled=True)
    token_range = jnp.arange(local_tokens, dtype=jnp.int32)
    combine = jnp.where(
        (source_index[None, :] == token_range[:, None]) & filled[None, :], seat_weight[None, :], 0.0
    )
    mixed_out = jnp.einsum(
        "tb,cb->tc",
        combine,
        returned.reshape(column_width, buffer_rows).astype(jnp.float32),
        precision=lax.Precision.HIGHEST,
    )
    return mixed_out.astype(jnp.bfloat16)


def solution(mesh):
    in_specs = (
        P("ep", None),
        P(),
        P(),
        P(),
        P(None, "ep", "tp"),
        P(None, "ep", "tp"),
        P(None, "ep", "tp"),
    )
    out_specs = P("ep", "tp")
    return jax.shard_map(body, mesh=mesh, in_specs=in_specs, out_specs=out_specs, check_vma=False)
```

profile of v0, /device:TPU:2, one launch (start us, length us, event | category | flops | bytes accessed | tf_op | source)
XLA Modules:
  0.0 386.7 jit_solution(5123035974095788254)
XLA Ops:
  6.5 1.1 convert_element_type.27
  7.7 1.2 multiply_reduce_fusion
  8.9 0.7 broadcast_compare_fusion
  9.6 0.8 convert_reduce_fusion.1
  10.5 0.2 select_reduce_fusion.2
  11.1 0.8 dynamic-slice
  12.0 2.0 gather_fusion
  14.1 20.3 %all_to_all.37 = bf16[8,64,512]{2,1,0:T(8,128)(2,1)} all-to-all(bf16[8,64,512]{2,1,0:T(8,128)(2,1)S(1)} %select_select_fusion), channel_id=1, replica_groups=mesh['ep'=8,'tp'=4] {'ep'}, dimensions={0} | all-to-all | bytes 1048576 | tf_op jit(solution)/shard_map/all_to_all | solution.py:56
  34.4 97.3 %all_to_all.38 = bf16[8,256,1024]{2,1,0:T(8,128)(2,1)} all-to-all(bf16[8,256,1024]{2,1,0:T(8,128)(2,1)} %param.11), channel_id=1, replica_groups=mesh['ep'=8,'tp'=4] {'ep'}, dimensions={0} | all-to-all | bytes 8388608 | tf_op jit(solution)/shard_map/all_to_all | solution.py:49
  131.8 96.2 %all_to_all.39 = bf16[8,256,1024]{2,1,0:T(8,128)(2,1)} all-to-all(bf16[8,256,1024]{2,1,0:T(8,128)(2,1)S(1)} %copy-done), channel_id=1, replica_groups=mesh['ep'=8,'tp'=4] {'ep'}, dimensions={0} | all-to-all | bytes 8388608 | tf_op jit(solution)/shard_map/all_to_all | solution.py:50
  228.0 4.5 %all-to-all-start.3 = ((bf16[8,256,1024]{2,1,0:T(8,128)(2,1)}), bf16[8,256,1024]{2,1,0:T(8,128)(2,1)}, u32[]{:S(2)}, u32[]{:S(2)}) async-start(bf16[8,256,1024]{2,1,0:T(8,128)(2,1)} %param.13), calls=%async_computation.3 | async-start | bytes 8388608 | tf_op jit(solution)/shard_map/all_to_all | solution.py:52
  232.6 0.7 all-gather.2.cloned.1.call-update
  233.3 0.7 and_select_fusion.1
  234.3 23.4 %all-gather.2.cloned.1.call-done = bf16[8,64,2048]{2,1,0:T(8,128)(2,1)} async-done(((bf16[8,64,512]{2,1,0:T(8,128)(2,1)}), bf16[8,64,2048]{2,1,0:T(8,128)(2,1)}) %all-gather.2.cloned.1.call-update) | async-done | bytes 2097168 | tf_op jit(solution)/shard_map/all_gather | solution.py:63
  257.7 4.2 %gather_fusion.1 = bf16[256,2048]{1,0:T(8,128)(2,1)S(1)} fusion(bf16[512,2048]{1,0:T(8,128)(2,1)} %bitcast.34, s32[1024]{0:T(1024)S(1)} %pad_clamp_fusion.1), kind=kCustom, calls=%fused_computation.1 | custom fusion | bytes 2098176 | tf_op jit(solution)/shard_map/jit(_take)/gather | solution.py:64
  261.9 3.5 fusion.5
  265.4 59.5 %all-to-all-done.3 = bf16[8,256,1024]{2,1,0:T(8,128)(2,1)} async-done(((bf16[8,256,1024]{2,1,0:T(8,128)(2,1)}), bf16[8,256,1024]{2,1,0:T(8,128)(2,1)}, u32[]{:S(2)}, u32[]{:S(2)}) %all-to-all-start.3) | async-done | bytes 4194336 | tf_op jit(solution)/shard_map/all_to_all | solution.py:52
  324.8 7.1 %fusion = bf16[2048,256]{0,1:T(8,128)(2,1)} fusion(bf16[2048,1024]{1,0:T(8,128)(2,1)} %bitcast.12, bf16[2048,1024]{1,0:T(8,128)(2,1)} %bitcast.35, f32[256,1024]{1,0:T(8,128)S(1)} %fusion.5, bf16[256,2048]{1,0:T(8,128)(2,1)S(1)} %gather_fusion.1, pred[256]{0:T(512)(128)(4,1)S(1)} %compare_and_fusion.2), kind=kOutput, calls=%fused_computation.4 | convolution fusion | flops 2150105088 | bytes 11534592 | tf_op jit(solution)/shard_map/df,bf->db/dot_general | solution.py:70
  332.3 22.6 %reduce-scatter.2.cloned.1.call-done = bf16[512,256]{0,1:T(8,128)(2,1)} async-done(((bf16[2048,256]{0,1:T(8,128)(2,1)}), bf16[512,256]{0,1:T(8,128)(2,1)}) %reduce-scatter.2.cloned.1.call-update) | async-done | bytes 262160 | tf_op jit(solution)/shard_map/reduce_scatter | solution.py:69
  354.8 3.0 gather_fusion.2
  357.8 0.9 broadcast_select_fusion.1
  358.7 5.7 %all-to-all-start.4 = ((bf16[512,8,64]{0,2,1:T(8,128)(2,1)}), bf16[512,8,64]{0,2,1:T(8,128)(2,1)S(1)}, u32[]{:S(2)}, u32[]{:S(2)}) async-start(bf16[512,8,64]{0,2,1:T(8,128)(2,1)} %broadcast_select_fusion.1), calls=%async_computation.5 | async-start | bytes 1048576 | tf_op jit(solution)/shard_map/all_to_all | solution.py:85
  364.9 13.9 %all-to-all-done.4 = bf16[512,8,64]{0,2,1:T(8,128)(2,1)S(1)} async-done(((bf16[512,8,64]{0,2,1:T(8,128)(2,1)}), bf16[512,8,64]{0,2,1:T(8,128)(2,1)S(1)}, u32[]{:S(2)}, u32[]{:S(2)}) %all-to-all-start.4) | async-done | bytes 524320 | tf_op jit(solution)/shard_map/all_to_all | solution.py:85
  378.8 1.0 convolution_convert_fusion.1
  (31 shorter events, 1.7 us)
Async XLA Ops:
  34.4 97.3 %copy-start = (bf16[8,256,1024]{2,1,0:T(8,128)(2,1)S(1)}, bf16[8,256,1024]{2,1,0:T(8,128)(2,1)}, u32[]{:S(2)}) copy-start(bf16[8,256,1024]{2,1,0:T(8,128)(2,1)} %param.12) | copy-start | bytes 12582916
  228.0 96.8 %all-to-all-start.3 = ((bf16[8,256,1024]{2,1,0:T(8,128)(2,1)}), bf16[8,256,1024]{2,1,0:T(8,128)(2,1)}, u32[]{:S(2)}, u32[]{:S(2)}) async-start(bf16[8,256,1024]{2,1,0:T(8,128)(2,1)} %param.13), calls=%async_computation.3 | async-start | bytes 8388608 | tf_op jit(solution)/shard_map/all_to_all | solution.py:52
  232.5 25.1 %all-gather.2.cloned.1.call-start = ((), (), s32[]{:S(2)}) async-start(), calls=%async_computation.6 | async-start | bytes 2621440 | tf_op jit(solution)/shard_map/all_gather | solution.py:63
  233.3 121.5 %reduce-scatter.2.cloned.1.call-start = ((), (), s32[]{:S(2)}) async-start(), calls=%async_computation.7 | async-start | bytes 1310720 | tf_op jit(solution)/shard_map/reduce_scatter | solution.py:69
  332.0 32.7 %copy-start.1 = (f32[8,256]{1,0:T(8,128)S(1)}, f32[8,256]{1,0:T(8,128)}, u32[]{:S(2)}) copy-start(f32[8,256]{1,0:T(8,128)} %param.10) | copy-start | bytes 24580
  358.7 20.1 %all-to-all-start.4 = ((bf16[512,8,64]{0,2,1:T(8,128)(2,1)}), bf16[512,8,64]{0,2,1:T(8,128)(2,1)S(1)}, u32[]{:S(2)}, u32[]{:S(2)}) async-start(bf16[512,8,64]{0,2,1:T(8,128)(2,1)} %broadcast_select_fusion.1), calls=%async_computation.5 | async-start | bytes 1048576 | tf_op jit(solution)/shard_map/all_to_all | solution.py:85
Sparse Core Ops, SparseCore 0:
  234.9 22.7 all-gather.1
  332.1 22.6 reduce-scatter.1
where the time goes:
time: 390 us; the launch traced here: 387 us
  blocking collectives  214 us (55%)
  waiting for transfers between devices  120 us (31%)
  between operations  13.6 us (3%)
  matrix products  11.6 us (3%)
  local copies, waits for them, and re-layouts  10.3 us (3%)
  starting transfers between devices  10.3 us (3%)
  other arithmetic  6.96 us (2%)
    all_to_all x1, blocking collectives, body(): lax.all_to_all(gate_send, 'ep', split_axis=0, concat_axis=1, tiled=True)  97.3 us
    all_to_all x1, blocking collectives, body(): lax.all_to_all(up_send, 'ep', split_axis=0, concat_axis=1, tiled=True)  96.2 us
    all_to_all x1, waiting for transfers between devices, body(): lax.all_to_all(down_send, 'ep', split_axis=0, concat_axis=1, tiled=True)  59.5 us
    all_gather x1, waiting for transfers between devices, body(): arrived = lax.all_gather(narrow, 'tp', axis=2, tiled=True)  23.4 us
    reduce_scatter x1, waiting for transfers between devices, body(): lax.psum_scatter(jnp.einsum('df,bf->db', down_rows, hidden, preferred_ele...  22.6 us
    all_to_all x1, blocking collectives, body(): lax.all_to_all(outgoing.reshape(expert_devices, seat_count, column_width)...  20.3 us
    all_to_all x1, waiting for transfers between devices, body(): lax.all_to_all(expert_out, 'ep', split_axis=1, concat_axis=1, tiled=True)  13.9 us
  transfers between devices with their start and end apart: 4, of which 4 were waited for; matrix products, arithmetic and copies ran while one was open for 2% of the time, Pallas kernels for 0%

commit v1 on v0

v1 whole, which is shorter than its diff:
```python
import functools

import jax
import jax.numpy as jnp
from jax import lax
from jax.experimental import pallas as pl
from jax.experimental.pallas import tpu as pltpu
from jax.sharding import PartitionSpec as P

EPSILON = 1e-06
MESH = pl.DeviceIdType.MESH
F32 = jnp.float32
BF16 = jnp.bfloat16


def kernel(
    n, n_tp, slots, tokens_ref, gain_ref, chosen_ref, weight_ref, gate_hbm, up_hbm, down_hbm, out_ref,
    gate_v, up_v, down_v, nbuf, xall, xs, sbuf, rbuf, hbuf, mix, obuf, fbuf,
    w_sem, d_send, d_recv, r_send, r_recv, g_send, g_recv, f_send, f_recv,
):
    experts, depth, ff = gate_v.shape
    rows = tokens_ref.shape[0]
    subs, width = sbuf.shape[1], sbuf.shape[3]
    half = subs // 2
    group = n // experts
    ratio = n // n_tp
    me = lax.axis_index("ep")
    col = lax.axis_index("tp")

    odd = me % 2
    pos = (1 - odd) * (me // 2) + odd * (n - 1 - me // 2)

    def index_at(position):
        p = (position + 2 * n) % n
        late = p // (n // 2)
        return (1 - late) * 2 * p + late * (2 * (n - 1 - p) + 1)

    neighbour = (index_at(pos + 1), index_at(pos - 1))
    owner_col = me // ratio
    own_slot = (me % ratio) * n_tp + col
    selfish = (owner_col == col).astype(jnp.int32)

    barrier = pltpu.get_barrier_semaphore()

    def greet(j, _):
        pl.semaphore_signal(barrier, inc=1, device_id=((me + j) % n, col), device_id_type=MESH)
        return 0

    lax.fori_loop(1, n, greet, 0)

    def greet_out(j, _):
        target = (me + j) % n
        source_row = col * ratio + j // n_tp
        source_col = j % n_tp

        @pl.when((target != me) | (owner_col != col))
        def _():
            pl.semaphore_signal(barrier, inc=1, device_id=(target, owner_col), device_id_type=MESH)

        @pl.when((source_row != me) | (source_col != col))
        def _():
            pl.semaphore_signal(barrier, inc=1, device_id=(source_row, source_col), device_id_type=MESH)

        return 0

    lax.fori_loop(0, n, greet_out, 0)

    loads = [
        pltpu.make_async_copy(gate_hbm, gate_v, w_sem.at[0]),
        pltpu.make_async_copy(up_hbm, up_v, w_sem.at[1]),
        pltpu.make_async_copy(down_hbm, down_v, w_sem.at[2]),
    ]
    for load in loads:
        load.start()

    values = tokens_ref[...].astype(F32)
    scale = lax.rsqrt(jnp.mean(values * values, axis=1, keepdims=True) + EPSILON)
    normed = (values * scale * gain_ref[...]).astype(BF16)
    for j in range(n):
        nbuf[j] = normed[:, j * depth : (j + 1) * depth]

    pl.semaphore_wait(barrier, (n - 1) + 2 * (n - selfish))

    def dispatch(target, source):
        return pltpu.make_async_remote_copy(
            src_ref=nbuf.at[target], dst_ref=xall.at[source], send_sem=d_send.at[target],
            recv_sem=d_recv.at[source], device_id=(target, col), device_id_type=MESH,
        )

    def send_tokens(j, _):
        dispatch((me + j) % n, me).start()
        return 0

    lax.fori_loop(1, n, send_tokens, 0)
    xall[me] = nbuf[me]
    mix[...] = jnp.zeros_like(mix)

    def wait_tokens(j, _):
        source = (me + n - j) % n
        pltpu.make_async_copy(nbuf.at[source], xall.at[source], d_recv.at[source]).wait()
        return 0

    lax.fori_loop(1, n, wait_tokens, 0)

    def piece_row(ref, q):
        start = pl.multiple_of((q % group) * slots, slots)
        return ref[pl.ds(q // group, 1), pl.ds(start, slots)]

    blocks = n * rows // 128
    step_blocks = min(blocks, 8)

    def gather(q):
        picked = jnp.transpose(jnp.broadcast_to(piece_row(chosen_ref, q), (128, slots)))
        lanes = lax.broadcasted_iota(jnp.int32, (slots, 128), 1)
        total = jnp.zeros((slots, depth), F32)
        per = step_blocks * 128 // rows
        for b in range(0, blocks, step_blocks):
            onehot = jnp.concatenate(
                [jnp.where(picked == lanes + (b + c) * 128, 1.0, 0.0).astype(BF16) for c in range(step_blocks)], axis=1
            )
            first = b * 128 // rows
            part = xall[first : first + per].reshape(step_blocks * 128, depth)
            total = total + jnp.dot(onehot, part, preferred_element_type=F32)
        xs[q] = total.astype(BF16)

    weights = (gate_v, up_v)

    def partial(direction, q, sub):
        w = weights[direction][q // group, :, sub * width : (sub + 1) * width]
        return jnp.dot(xs[q], w, preferred_element_type=F32)

    def reduce_copy(direction, src, step, sub):
        return pltpu.make_async_remote_copy(
            src_ref=src, dst_ref=rbuf.at[direction, step, sub], send_sem=r_send.at[direction, step, sub],
            recv_sem=r_recv.at[direction, step, sub], device_id=(neighbour[direction], col), device_id_type=MESH,
        )

    def chunk(direction, step):
        return index_at(pos - 1 - step) if direction == 0 else index_at(pos + 1 + step)

    gather(chunk(0, 0))
    gather(chunk(1, 0))
    loads[0].wait()
    loads[1].wait()
    for sub in range(subs):
        for direction in range(2):
            sbuf[direction, sub] = partial(direction, chunk(direction, 0), sub).astype(BF16)
            reduce_copy(direction, sbuf.at[direction, sub], 0, sub).start()

    def gather_rest(j, _):
        gather(index_at(pos - 1 - j))
        return 0

    lax.fori_loop(1, n - 2, gather_rest, 0)
    gather(me)

    def reduce_step(step, _):
        for sub in range(subs):
            for direction in range(2):
                mine = partial(direction, chunk(direction, step), sub)
                here = rbuf.at[direction, step - 1, sub]
                reduce_copy(direction, here, step - 1, sub).wait_recv()
                here[...] = (here[...].astype(F32) + mine).astype(BF16)
                reduce_copy(direction, here, step, sub).start()
        return 0

    lax.fori_loop(1, n - 1, reduce_step, 0)

    def spread_copy(direction, source, step, sub):
        block = hbuf.at[source, sub]
        return pltpu.make_async_remote_copy(
            src_ref=block, dst_ref=block, send_sem=g_send.at[step, sub], recv_sem=g_recv.at[step, sub],
            device_id=(neighbour[direction], col), device_id_type=MESH,
        )

    slot_scale = jnp.transpose(jnp.broadcast_to(piece_row(weight_ref, me), (128, slots)))
    slot_scale = jnp.concatenate([slot_scale] * (width // 128), axis=1)
    order = [s for pair in zip(range(half), range(half, subs)) for s in pair]
    for sub in order:
        parts = []
        for direction in range(2):
            mine = partial(direction, me, sub)
            here = rbuf.at[direction, n - 2, sub]
            reduce_copy(direction, here, n - 2, sub).wait_recv()
            parts.append(here[...].astype(F32) + mine)
        hbuf[me, sub] = (parts[0] / (1.0 + jnp.exp(-parts[0])) * parts[1] * slot_scale).astype(BF16)
        spread_copy(sub // half, me, 0, sub).start()
    loads[2].wait()

    def project(q, direction):
        total = jnp.zeros((slots, depth), F32)
        for sub in range(direction * half, (direction + 1) * half):
            w = down_v[q // group, :, sub * width : (sub + 1) * width]
            total = total + lax.dot_general(
                hbuf[q, sub], w, (((1,), (1,)), ((), ())), preferred_element_type=F32
            )
        picked = piece_row(chosen_ref, q)
        value = total.astype(BF16)
        size = step_blocks * 128
        for b in range(0, n * rows, size):
            numbers = lax.broadcasted_iota(jnp.int32, (size, slots), 0) + b
            onehot = jnp.where(numbers == picked, 1.0, 0.0).astype(BF16)
            mix[b : b + size] += jnp.dot(onehot, value, preferred_element_type=F32)

    project(me, 0)
    project(me, 1)

    def spread_step(step, _):
        for direction in range(2):
            source = chunk(direction, step - 1)
            for sub in range(direction * half, (direction + 1) * half):
                spread_copy(direction, source, step - 1, sub).wait_recv()

                @pl.when(step < n - 1)
                def _():
                    spread_copy(direction, source, step, sub).start()

        for direction in range(2):
            project(chunk(direction, step - 1), direction)
        return 0

    lax.fori_loop(1, n, spread_step, 0)

    def final_copy(target, slot):
        return pltpu.make_async_remote_copy(
            src_ref=obuf.at[target], dst_ref=fbuf.at[slot], send_sem=f_send.at[target],
            recv_sem=f_recv.at[slot], device_id=(target, owner_col), device_id_type=MESH,
        )

    def send_out(j, _):
        target = (me + j) % n
        start = pl.multiple_of(target * rows, rows)
        obuf[target] = mix[pl.ds(start, rows), :].astype(BF16)
        away = (target != me) | (owner_col != col)

        @pl.when(away)
        def _():
            final_copy(target, own_slot).start()

        @pl.when(jnp.logical_not(away))
        def _():
            fbuf[own_slot] = obuf[target]

        return 0

    lax.fori_loop(0, n, send_out, 0)

    def sent_tokens(j, _):
        dispatch((me + j) % n, me).wait_send()
        return 0

    lax.fori_loop(1, n, sent_tokens, 0)

    def sent_ring(step, _):
        for sub in range(subs):
            for direction in range(2):
                reduce_copy(direction, sbuf.at[direction, sub], step, sub).wait_send()
            spread_copy(sub // half, me, step, sub).wait_send()
        return 0

    lax.fori_loop(0, n - 1, sent_ring, 0)

    def arrive(j, _):
        source_row = col * ratio + j // n_tp
        source_col = j % n_tp

        @pl.when((source_row != me) | (source_col != col))
        def _():
            pltpu.make_async_copy(obuf.at[0], fbuf.at[j], f_recv.at[j]).wait()

        return 0

    lax.fori_loop(0, n, arrive, 0)
    for b in range(ratio):
        total = fbuf[b * n_tp].astype(F32)
        for k in range(1, n_tp):
            total = total + fbuf[b * n_tp + k].astype(F32)
        out_ref[:, b * depth : (b + 1) * depth] = total.astype(BF16)

    def sent_out(j, _):
        target = (me + j) % n

        @pl.when((target != me) | (owner_col != col))
        def _():
            final_copy(target, own_slot).wait_send()

        return 0

    lax.fori_loop(0, n, sent_out, 0)


def body(tokens, norm_gain, chosen, slot_weight, gate_weight, up_weight, down_weight):
    n = lax.axis_size("ep")
    n_tp = lax.axis_size("tp")
    rows, model_width = tokens.shape
    experts, depth, ff = gate_weight.shape
    slots = chosen.shape[0] * chosen.shape[1] // n
    width = max(128, ff // 4)
    subs = ff // width
    vmem = pl.BlockSpec(memory_space=pltpu.VMEM)
    anywhere = pl.BlockSpec(memory_space=pl.ANY)
    dma = pltpu.SemaphoreType.DMA
    return pl.pallas_call(
        functools.partial(kernel, n, n_tp, slots),
        out_shape=jax.ShapeDtypeStruct((rows, model_width // n_tp), BF16),
        in_specs=[vmem] * 4 + [anywhere] * 3,
        out_specs=vmem,
        scratch_shapes=[
            pltpu.VMEM((experts, depth, ff), BF16),
            pltpu.VMEM((experts, depth, ff), BF16),
            pltpu.VMEM((experts, depth, ff), BF16),
            pltpu.VMEM((n, rows, depth), BF16),
            pltpu.VMEM((n, rows, depth), BF16),
            pltpu.VMEM((n, slots, depth), BF16),
            pltpu.VMEM((2, subs, slots, width), BF16),
            pltpu.VMEM((2, n - 1, subs, slots, width), BF16),
            pltpu.VMEM((n, subs, slots, width), BF16),
            pltpu.VMEM((n * rows, depth), F32),
            pltpu.VMEM((n, rows, depth), BF16),
            pltpu.VMEM((n, rows, depth), BF16),
            dma((3,)),
            dma((n,)),
            dma((n,)),
            dma((2, n - 1, subs)),
            dma((2, n - 1, subs)),
            dma((n - 1, subs)),
            dma((n - 1, subs)),
            dma((n,)),
            dma((n,)),
        ],
        compiler_params=pltpu.CompilerParams(
            collective_id=0, has_side_effects=True, vmem_limit_bytes=64 * 1024 * 1024 - 96 * 1024
        ),
    )(tokens, norm_gain.reshape(1, model_width), chosen, slot_weight, gate_weight, up_weight, down_weight)


def solution(mesh):
    in_specs = (
        P("ep", None),
        P(),
        P(),
        P(),
        P(None, "ep", "tp"),
        P(None, "ep", "tp"),
        P(None, "ep", "tp"),
    )
    out_specs = P("ep", "tp")
    return jax.shard_map(body, mesh=mesh, in_specs=in_specs, out_specs=out_specs, check_vma=False)
```

time: 390 us -> 157 us (0.40)
  blocking collectives: 214 us -> 0 us
  Pallas kernels: 0 us -> 152 us
  waiting for transfers between devices: 120 us -> 0 us
  between operations: 13.6 us -> 0.01 us
  matrix products: 11.6 us -> 0 us
  starting transfers between devices: 10.3 us -> 0 us
  local copies, waits for them, and re-layouts: 10.3 us -> 1.57 us
  other arithmetic: 6.96 us -> 0 us
    all_to_all x3 -> x0, blocking collectives: 214 us -> none  [the longest x1 97.3 us: body(): lax.all_to_all(gate_send, 'ep', split_axis=0, concat_axis=1, tiled=True)]
    pallas_call x0 -> x1, Pallas kernels: none -> 152 us  [body(): pl.pallas_call(functools.partial(kernel, n, n_tp, slots), out_shape=jax.S...]
    all_to_all x2 -> x0, waiting for transfers between devices: 73.4 us -> none  [the longest x1 59.5 us: body(): lax.all_to_all(down_send, 'ep', split_axis=0, concat_axis=1, tiled=True)]
    all_gather x1 -> x0, waiting for transfers between devices: 23.4 us -> none  [body(): arrived = lax.all_gather(narrow, 'tp', axis=2, tiled=True)]
    reduce_scatter x1 -> x0, waiting for transfers between devices: 22.6 us -> none  [body(): lax.psum_scatter(jnp.einsum('df,bf->db', down_rows, hidden, preferred_ele...]
    dot_general x3 -> x0, matrix products: 11.6 us -> none  [the longest x1 7.12 us: body(): jnp.einsum('df,bf->db', down_rows, hidden, preferred_element_type=jnp.flo...]
    all_to_all x2 -> x0, starting transfers between devices: 10.3 us -> none  [the longest x1 5.71 us: body(): lax.all_to_all(expert_out, 'ep', split_axis=1, concat_axis=1, tiled=True)]
    gather x3 -> x0, local copies, waits for them, and re-layouts: 9.16 us -> none  [the longest x1 4.22 us: body(): jnp.take(arrived.reshape(buffer_rows, model_width), arrival_row, axis=0)]
  transfers between devices with their start and end apart: 4 -> 0, of which waited for: 4 -> 0; matrix products, arithmetic and copies ran while one was open for 2% -> 0% of each run, Pallas kernels for 0% -> 0%
where the time goes in v1:
time: 157 us; the launch traced here: 154 us
  Pallas kernels  152 us (97%)
  local copies, waits for them, and re-layouts  1.57 us (1%)
    pallas_call x1, Pallas kernels, body(): pl.pallas_call(functools.partial(kernel, n, n_tp, slots), out_shape=jax.S...  152 us

profile of v1, /device:TPU:2, one launch (start us, length us, event | category | flops | bytes accessed | tf_op | source)
XLA Modules:
  0.0 153.9 jit_solution(13379152073202053988)
XLA Ops:
  0.0 152.3 %shard_map.73 = bf16[128,512]{1,0:T(8,128)(2,1)} custom-call(bf16[128,2048]{1,0:T(8,128)(2,1)} %tokens_ref.1, f32[1,2048]{1,0:T(1,128)} %bitcast.1, s32[8,256]{1,0:T(8,128)} %chosen_ref.1, f32[8,256]{1,0:T(8,128)} %weight_ref.1, bf16[8,256,1024]{2,1,0:T(8,128)(2,1)} %gate_hbm.1, bf16[8,256,1024]{2,1,0:T(8,128)(2,1)} %up_hbm.1, bf16[8,256,1024]{2,1,0:T(8,128)(2,1)} %down_hbm.1), custom_call_target="tpu_custom_call" | custom-call | tf_op jit(solution)/shard_map/pallas_call | solution.py:303
  152.3 1.6 %copy.9 = bf16[128,512]{1,0:T(8,128)(2,1)} copy(bf16[128,512]{1,0:T(8,128)(2,1)} %shard_map.73) | data formatting | bytes 262144

commit v2 on v1

--- a/solution.py
+++ b/solution.py
@@ -15,8 +15,8 @@
 
 def kernel(
     n, n_tp, slots, tokens_ref, gain_ref, chosen_ref, weight_ref, gate_hbm, up_hbm, down_hbm, out_ref,
-    gate_v, up_v, down_v, nbuf, xall, xs, sbuf, rbuf, hbuf, mix, obuf, fbuf,
-    w_sem, d_send, d_recv, r_send, r_recv, g_send, g_recv, f_send, f_recv,
+    gate_v, up_v, down_v, nbuf, xall, xs, sbuf, rbuf, hbuf, mix, obuf, pbuf, sumbuf, fbuf,
+    w_sem, d_send, d_recv, c_send, c_recv, r_send, r_recv, g_send, g_recv, p_send, p_recv, f_send, f_recv,
 ):
     experts, depth, ff = gate_v.shape
     rows = tokens_ref.shape[0]
@@ -37,8 +37,12 @@
 
     neighbour = (index_at(pos + 1), index_at(pos - 1))
     owner_col = me // ratio
-    own_slot = (me % ratio) * n_tp + col
-    selfish = (owner_col == col).astype(jnp.int32)
+    core = col % 2
+    partner = col + 1 - 2 * core
+    pairs = n_tp // 2
+    own_slot = (me % ratio) * pairs + col // 2
+    part_rows = rows // 2
+    selfish = ((owner_col == col) & (me % 2 == core)).astype(jnp.int32)
 
     barrier = pltpu.get_barrier_semaphore()
 
@@ -48,10 +52,17 @@
 
     lax.fori_loop(1, n, greet, 0)
 
+    pl.semaphore_signal(barrier, inc=1, device_id=(me, partner), device_id_type=MESH)
+
+    def owner_at(j):
+        return ((me // 2 + j) % (n // 2)) * 2 + core
+
+    def source_at(j):
+        return col * ratio + j // pairs, (j % pairs) * 2 + me % 2
+
     def greet_out(j, _):
-        target = (me + j) % n
-        source_row = col * ratio + j // n_tp
-        source_col = j % n_tp
+        target = owner_at(j)
+        source_row, source_col = source_at(j)
 
         @pl.when((target != me) | (owner_col != col))
         def _():
@@ -63,7 +74,7 @@
 
         return 0
 
-    lax.fori_loop(0, n, greet_out, 0)
+    lax.fori_loop(0, n // 2, greet_out, 0)
 
     loads = [
         pltpu.make_async_copy(gate_hbm, gate_v, w_sem.at[0]),
@@ -73,18 +84,25 @@
     for load in loads:
         load.start()
 
-    values = tokens_ref[...].astype(F32)
+    my_rows = pl.ds(pl.multiple_of(core * part_rows, part_rows), part_rows)
+    values = tokens_ref[my_rows, :].astype(F32)
     scale = lax.rsqrt(jnp.mean(values * values, axis=1, keepdims=True) + EPSILON)
     normed = (values * scale * gain_ref[...]).astype(BF16)
     for j in range(n):
         nbuf[j] = normed[:, j * depth : (j + 1) * depth]
 
-    pl.semaphore_wait(barrier, (n - 1) + 2 * (n - selfish))
+    pl.semaphore_wait(barrier, n + 2 * (n // 2 - selfish))
 
     def dispatch(target, source):
         return pltpu.make_async_remote_copy(
-            src_ref=nbuf.at[target], dst_ref=xall.at[source], send_sem=d_send.at[target],
+            src_ref=nbuf.at[target], dst_ref=xall.at[source, core], send_sem=d_send.at[target],
             recv_sem=d_recv.at[source], device_id=(target, col), device_id_type=MESH,
+        )
+
+    def share(src, source, half_index):
+        return pltpu.make_async_remote_copy(
+            src_ref=src, dst_ref=xall.at[source, half_index], send_sem=c_send.at[source],
+            recv_sem=c_recv.at[source], device_id=(me, partner), device_id_type=MESH,
         )
 
     def send_tokens(j, _):
@@ -92,15 +110,24 @@
         return 0
 
     lax.fori_loop(1, n, send_tokens, 0)
-    xall[me] = nbuf[me]
+    share(nbuf.at[me], me, core).start()
+    xall[me, core] = nbuf[me]
     mix[...] = jnp.zeros_like(mix)
+
+    def pass_tokens(j, _):
+        source = (me + n - j) % n
+        dispatch(me, source).wait_recv()
+        share(xall.at[source, core], source, core).start()
+        return 0
+
+    lax.fori_loop(1, n, pass_tokens, 0)
 
     def wait_tokens(j, _):
         source = (me + n - j) % n
-        pltpu.make_async_copy(nbuf.at[source], xall.at[source], d_recv.at[source]).wait()
-        return 0
-
-    lax.fori_loop(1, n, wait_tokens, 0)
+        share(xall.at[source, core], source, 1 - core).wait_recv()
+        return 0
+
+    lax.fori_loop(0, n, wait_tokens, 0)
 
     def piece_row(ref, q):
         start = pl.multiple_of((q % group) * slots, slots)
@@ -221,35 +248,57 @@
 
     lax.fori_loop(1, n, spread_step, 0)
 
-    def final_copy(target, slot):
-        return pltpu.make_async_remote_copy(
-            src_ref=obuf.at[target], dst_ref=fbuf.at[slot], send_sem=f_send.at[target],
-            recv_sem=f_recv.at[slot], device_id=(target, owner_col), device_id_type=MESH,
-        )
+    def pair_copy(j):
+        return pltpu.make_async_remote_copy(
+            src_ref=obuf.at[j], dst_ref=pbuf.at[j], send_sem=p_send.at[j],
+            recv_sem=p_recv.at[j], device_id=(me, partner), device_id_type=MESH,
+        )
+
+    def final_copy(j, slot):
+        return pltpu.make_async_remote_copy(
+            src_ref=sumbuf.at[j], dst_ref=fbuf.at[slot], send_sem=f_send.at[j],
+            recv_sem=f_recv.at[slot], device_id=(owner_at(j), owner_col), device_id_type=MESH,
+        )
+
+    def mix_rows(target):
+        return mix[pl.ds(pl.multiple_of(target * rows, rows), rows), :]
+
+    def send_pair(j, _):
+        obuf[j] = mix_rows(owner_at(j) + 1 - 2 * core).astype(BF16)
+        pair_copy(j).start()
+        return 0
+
+    lax.fori_loop(0, n // 2, send_pair, 0)
 
     def send_out(j, _):
-        target = (me + j) % n
-        start = pl.multiple_of(target * rows, rows)
-        obuf[target] = mix[pl.ds(start, rows), :].astype(BF16)
+        target = owner_at(j)
+        pair_copy(j).wait_recv()
+        sumbuf[j] = (mix_rows(target) + pbuf[j].astype(F32)).astype(BF16)
         away = (target != me) | (owner_col != col)
 
         @pl.when(away)
         def _():
-            final_copy(target, own_slot).start()
+            final_copy(j, own_slot).start()
 
         @pl.when(jnp.logical_not(away))
         def _():
-            fbuf[own_slot] = obuf[target]
-
-        return 0
-
-    lax.fori_loop(0, n, send_out, 0)
+            fbuf[own_slot] = sumbuf[j]
+
+        return 0
+
+    lax.fori_loop(0, n // 2, send_out, 0)
 
     def sent_tokens(j, _):
-        dispatch((me + j) % n, me).wait_send()
-        return 0
-
-    lax.fori_loop(1, n, sent_tokens, 0)
+        source = (me + j) % n
+        share(xall.at[source, core], source, core).wait_send()
+
+        @pl.when(j > 0)
+        def _():
+            dispatch(source, me).wait_send()
+
+        return 0
+
+    lax.fori_loop(0, n, sent_tokens, 0)
 
     def sent_ring(step, _):
         for sub in range(subs):
@@ -261,32 +310,31 @@
     lax.fori_loop(0, n - 1, sent_ring, 0)
 
     def arrive(j, _):
-        source_row = col * ratio + j // n_tp
-        source_col = j % n_tp
+        source_row, source_col = source_at(j)
 
         @pl.when((source_row != me) | (source_col != col))
         def _():
-            pltpu.make_async_copy(obuf.at[0], fbuf.at[j], f_recv.at[j]).wait()
-
-        return 0
-
-    lax.fori_loop(0, n, arrive, 0)
+            final_copy(0, j).wait_recv()
+
+        return 0
+
+    lax.fori_loop(0, n // 2, arrive, 0)
     for b in range(ratio):
-        total = fbuf[b * n_tp].astype(F32)
-        for k in range(1, n_tp):
-            total = total + fbuf[b * n_tp + k].astype(F32)
+        total = fbuf[b * pairs].astype(F32)
+        for k in range(1, pairs):
+            total = total + fbuf[b * pairs + k].astype(F32)
         out_ref[:, b * depth : (b + 1) * depth] = total.astype(BF16)
 
     def sent_out(j, _):
-        target = (me + j) % n
-
-        @pl.when((target != me) | (owner_col != col))
-        def _():
-            final_copy(target, own_slot).wait_send()
-
-        return 0
-
-    lax.fori_loop(0, n, sent_out, 0)
+        pair_copy(j).wait_send()
+
+        @pl.when((owner_at(j) != me) | (owner_col != col))
+        def _():
+            final_copy(j, own_slot).wait_send()
+
+        return 0
+
+    lax.fori_loop(0, n // 2, sent_out, 0)
 
 
 def body(tokens, norm_gain, chosen, slot_weight, gate_weight, up_weight, down_weight):
@@ -309,24 +357,30 @@
             pltpu.VMEM((experts, depth, ff), BF16),
             pltpu.VMEM((experts, depth, ff), BF16),
             pltpu.VMEM((experts, depth, ff), BF16),
-            pltpu.VMEM((n, rows, depth), BF16),
-            pltpu.VMEM((n, rows, depth), BF16),
+            pltpu.VMEM((n, rows // 2, depth), BF16),
+            pltpu.VMEM((n, 2, rows // 2, depth), BF16),
             pltpu.VMEM((n, slots, depth), BF16),
             pltpu.VMEM((2, subs, slots, width), BF16),
             pltpu.VMEM((2, n - 1, subs, slots, width), BF16),
             pltpu.VMEM((n, subs, slots, width), BF16),
             pltpu.VMEM((n * rows, depth), F32),
-            pltpu.VMEM((n, rows, depth), BF16),
-            pltpu.VMEM((n, rows, depth), BF16),
+            pltpu.VMEM((n // 2, rows, depth), BF16),
+            pltpu.VMEM((n // 2, rows, depth), BF16),
+            pltpu.VMEM((n // 2, rows, depth), BF16),
+            pltpu.VMEM((n // 2, rows, depth), BF16),
             dma((3,)),
+            dma((n,)),
+            dma((n,)),
             dma((n,)),
             dma((n,)),
             dma((2, n - 1, subs)),
             dma((2, n - 1, subs)),
             dma((n - 1, subs)),
             dma((n - 1, subs)),
-            dma((n,)),
-            dma((n,)),
+            dma((n // 2,)),
+            dma((n // 2,)),
+            dma((n // 2,)),
+            dma((n // 2,)),
         ],
         compiler_params=pltpu.CompilerParams(
             collective_id=0, has_side_effects=True, vmem_limit_bytes=64 * 1024 * 1024 - 96 * 1024

time: 157 us -> 150 us (0.955)
  Pallas kernels: 152 us -> 147 us
    pallas_call x1, Pallas kernels: 152 us -> 147 us  [body(): pl.pallas_call(functools.partial(kernel, n, n_tp, slots), out_shape=jax.S...]
where the time goes in v2:
time: 150 us; the launch traced here: 148 us
  Pallas kernels  147 us (98%)
  local copies, waits for them, and re-layouts  1.57 us (1%)
    pallas_call x1, Pallas kernels, body(): pl.pallas_call(functools.partial(kernel, n, n_tp, slots), out_shape=jax.S...  147 us

profile of v2, /device:TPU:2, one launch (start us, length us, event | category | flops | bytes accessed | tf_op | source)
XLA Modules:
  0.0 148.2 jit_solution(14840371455836743208)
XLA Ops:
  0.0 146.6 %shard_map.73 = bf16[128,512]{1,0:T(8,128)(2,1)} custom-call(bf16[128,2048]{1,0:T(8,128)(2,1)} %tokens_ref.1, f32[1,2048]{1,0:T(1,128)} %bitcast.1, s32[8,256]{1,0:T(8,128)} %chosen_ref.1, f32[8,256]{1,0:T(8,128)} %weight_ref.1, bf16[8,256,1024]{2,1,0:T(8,128)(2,1)} %gate_hbm.1, bf16[8,256,1024]{2,1,0:T(8,128)(2,1)} %up_hbm.1, bf16[8,256,1024]{2,1,0:T(8,128)(2,1)} %down_hbm.1), custom_call_target="tpu_custom_call" | custom-call | tf_op jit(solution)/shard_map/pallas_call | solution.py:351
  146.6 1.6 %copy.9 = bf16[128,512]{1,0:T(8,128)(2,1)} copy(bf16[128,512]{1,0:T(8,128)(2,1)} %shard_map.73) | data formatting | bytes 262144

commit v3 on v2

--- a/solution.py
+++ b/solution.py
@@ -55,7 +55,7 @@
     pl.semaphore_signal(barrier, inc=1, device_id=(me, partner), device_id_type=MESH)
 
     def owner_at(j):
-        return ((me // 2 + j) % (n // 2)) * 2 + core
+        return ((me // 2 + n // 2 - 1 - j) % (n // 2)) * 2 + core
 
     def source_at(j):
         return col * ratio + j // pairs, (j % pairs) * 2 + me % 2
@@ -105,22 +105,26 @@
             recv_sem=c_recv.at[source], device_id=(me, partner), device_id_type=MESH,
         )
 
+    def offset(j):
+        late = j // (n // 2)
+        return (1 - late) * (n // 2 + j) + late * (n - 1 - j)
+
     def send_tokens(j, _):
-        dispatch((me + j) % n, me).start()
-        return 0
-
-    lax.fori_loop(1, n, send_tokens, 0)
+        dispatch((me + offset(j)) % n, me).start()
+        return 0
+
+    lax.fori_loop(0, n - 1, send_tokens, 0)
     share(nbuf.at[me], me, core).start()
     xall[me, core] = nbuf[me]
     mix[...] = jnp.zeros_like(mix)
 
     def pass_tokens(j, _):
-        source = (me + n - j) % n
+        source = (me + n - offset(j)) % n
         dispatch(me, source).wait_recv()
         share(xall.at[source, core], source, core).start()
         return 0
 
-    lax.fori_loop(1, n, pass_tokens, 0)
+    lax.fori_loop(0, n - 1, pass_tokens, 0)
 
     def wait_tokens(j, _):
         source = (me + n - j) % n
@@ -165,12 +169,12 @@
     def chunk(direction, step):
         return index_at(pos - 1 - step) if direction == 0 else index_at(pos + 1 + step)
 
-    gather(chunk(0, 0))
-    gather(chunk(1, 0))
     loads[0].wait()
     loads[1].wait()
     for sub in range(subs):
         for direction in range(2):
+            if sub == 0:
+                gather(chunk(direction, 0))
             sbuf[direction, sub] = partial(direction, chunk(direction, 0), sub).astype(BF16)
             reduce_copy(direction, sbuf.at[direction, sub], 0, sub).start()
 
@@ -214,39 +218,54 @@
         spread_copy(sub // half, me, 0, sub).start()
     loads[2].wait()
 
-    def project(q, direction):
+    def down(q, direction):
         total = jnp.zeros((slots, depth), F32)
         for sub in range(direction * half, (direction + 1) * half):
             w = down_v[q // group, :, sub * width : (sub + 1) * width]
             total = total + lax.dot_general(
                 hbuf[q, sub], w, (((1,), (1,)), ((), ())), preferred_element_type=F32
             )
+        return total.astype(BF16)
+
+    def project(q, direction):
         picked = piece_row(chosen_ref, q)
-        value = total.astype(BF16)
+        value = down(q, direction)
         size = step_blocks * 128
         for b in range(0, n * rows, size):
             numbers = lax.broadcasted_iota(jnp.int32, (size, slots), 0) + b
             onehot = jnp.where(numbers == picked, 1.0, 0.0).astype(BF16)
             mix[b : b + size] += jnp.dot(onehot, value, preferred_element_type=F32)
 
-    project(me, 0)
-    project(me, 1)
-
     def spread_step(step, _):
-        for direction in range(2):
-            source = chunk(direction, step - 1)
-            for sub in range(direction * half, (direction + 1) * half):
+        for t in range(half):
+            for direction in range(2):
+                sub = direction * half + t
+                source = chunk(direction, step - 1)
                 spread_copy(direction, source, step - 1, sub).wait_recv()
 
                 @pl.when(step < n - 1)
                 def _():
                     spread_copy(direction, source, step, sub).start()
 
-        for direction in range(2):
-            project(chunk(direction, step - 1), direction)
+            for direction in range(2):
+                if direction % half == t:
+                    project(chunk(direction, step - 2), direction)
         return 0
 
     lax.fori_loop(1, n, spread_step, 0)
+
+    last = (chunk(0, n - 2), chunk(1, n - 2))
+    for direction in range(2):
+        xs[direction] = down(last[direction], direction)
+
+    def mix_rows(target):
+        start = pl.multiple_of(target * rows, rows)
+        numbers = lax.broadcasted_iota(jnp.int32, (rows, slots), 0) + start
+        onehot = jnp.concatenate(
+            [jnp.where(numbers == piece_row(chosen_ref, q), 1.0, 0.0).astype(BF16) for q in last], axis=1
+        )
+        late = jnp.dot(onehot, xs[0:2].reshape(2 * slots, depth), preferred_element_type=F32)
+        return mix[pl.ds(start, rows), :] + late
 
     def pair_copy(j):
         return pltpu.make_async_remote_copy(
@@ -259,9 +278,6 @@
             src_ref=sumbuf.at[j], dst_ref=fbuf.at[slot], send_sem=f_send.at[j],
             recv_sem=f_recv.at[slot], device_id=(owner_at(j), owner_col), device_id_type=MESH,
         )
-
-    def mix_rows(target):
-        return mix[pl.ds(pl.multiple_of(target * rows, rows), rows), :]
 
     def send_pair(j, _):
         obuf[j] = mix_rows(owner_at(j) + 1 - 2 * core).astype(BF16)

time: 150 us -> 151 us (level); the launches traced: 148 us -> 151 us
  Pallas kernels: 147 us -> 149 us
    pallas_call x1, Pallas kernels: 147 us -> 149 us  [body(): pl.pallas_call(functools.partial(kernel, n, n_tp, slots), out_shape=jax.S...]
where the time goes in v3:
time: 151 us
  Pallas kernels  149 us (99%)
  local copies, waits for them, and re-layouts  1.57 us (1%)
    pallas_call x1, Pallas kernels, body(): pl.pallas_call(functools.partial(kernel, n, n_tp, slots), out_shape=jax.S...  149 us

profile of v3, /device:TPU:2, one launch (start us, length us, event | category | flops | bytes accessed | tf_op | source)
XLA Modules:
  0.0 150.8 jit_solution(14817304682533246302)
XLA Ops:
  0.0 149.3 %shard_map.73 = bf16[128,512]{1,0:T(8,128)(2,1)} custom-call(bf16[128,2048]{1,0:T(8,128)(2,1)} %tokens_ref.1, f32[1,2048]{1,0:T(1,128)} %bitcast.1, s32[8,256]{1,0:T(8,128)} %chosen_ref.1, f32[8,256]{1,0:T(8,128)} %weight_ref.1, bf16[8,256,1024]{2,1,0:T(8,128)(2,1)} %gate_hbm.1, bf16[8,256,1024]{2,1,0:T(8,128)(2,1)} %up_hbm.1, bf16[8,256,1024]{2,1,0:T(8,128)(2,1)} %down_hbm.1), custom_call_target="tpu_custom_call" | custom-call | tf_op jit(solution)/shard_map/pallas_call | solution.py:367
  149.3 1.6 %copy.9 = bf16[128,512]{1,0:T(8,128)(2,1)} copy(bf16[128,512]{1,0:T(8,128)(2,1)} %shard_map.73) | data formatting | bytes 262144

commit v4 on v3

--- a/solution.py
+++ b/solution.py
@@ -197,10 +197,13 @@
 
     lax.fori_loop(1, n - 1, reduce_step, 0)
 
-    def spread_copy(direction, source, step, sub):
-        block = hbuf.at[source, sub]
-        return pltpu.make_async_remote_copy(
-            src_ref=block, dst_ref=block, send_sem=g_send.at[step, sub], recv_sem=g_recv.at[step, sub],
+    bands = 2
+    band_rows = slots // bands
+
+    def spread_copy(direction, source, step, sub, band):
+        block = hbuf.at[source, sub, pl.ds(band * band_rows, band_rows)]
+        return pltpu.make_async_remote_copy(
+            src_ref=block, dst_ref=block, send_sem=g_send.at[step, sub, band], recv_sem=g_recv.at[step, sub, band],
             device_id=(neighbour[direction], col), device_id_type=MESH,
         )
 
@@ -215,7 +218,8 @@
             reduce_copy(direction, here, n - 2, sub).wait_recv()
             parts.append(here[...].astype(F32) + mine)
         hbuf[me, sub] = (parts[0] / (1.0 + jnp.exp(-parts[0])) * parts[1] * slot_scale).astype(BF16)
-        spread_copy(sub // half, me, 0, sub).start()
+        for band in range(bands):
+            spread_copy(sub // half, me, 0, sub, band).start()
     loads[2].wait()
 
     def down(q, direction):
@@ -238,14 +242,14 @@
 
     def spread_step(step, _):
         for t in range(half):
-            for direction in range(2):
+            for band, direction in ((0, 0), (0, 1), (1, 0), (1, 1)):
                 sub = direction * half + t
                 source = chunk(direction, step - 1)
-                spread_copy(direction, source, step - 1, sub).wait_recv()
+                spread_copy(direction, source, step - 1, sub, band).wait_recv()
 
                 @pl.when(step < n - 1)
                 def _():
-                    spread_copy(direction, source, step, sub).start()
+                    spread_copy(direction, source, step, sub, band).start()
 
             for direction in range(2):
                 if direction % half == t:
@@ -320,7 +324,8 @@
         for sub in range(subs):
             for direction in range(2):
                 reduce_copy(direction, sbuf.at[direction, sub], step, sub).wait_send()
-            spread_copy(sub // half, me, step, sub).wait_send()
+            for band in range(bands):
+                spread_copy(sub // half, me, step, sub, band).wait_send()
         return 0
 
     lax.fori_loop(0, n - 1, sent_ring, 0)
@@ -391,8 +396,8 @@
             dma((n,)),
             dma((2, n - 1, subs)),
             dma((2, n - 1, subs)),
-            dma((n - 1, subs)),
-            dma((n - 1, subs)),
+            dma((n - 1, subs, 2)),
+            dma((n - 1, subs, 2)),
             dma((n // 2,)),
             dma((n // 2,)),
             dma((n // 2,)),

time: 151 us -> 151 us (level)
  no operation moved by 1% of the time
where the time goes in v4:
time: 151 us
  Pallas kernels  150 us (99%)
  local copies, waits for them, and re-layouts  1.57 us (1%)
    pallas_call x1, Pallas kernels, body(): pl.pallas_call(functools.partial(kernel, n, n_tp, slots), out_shape=jax.S...  150 us

profile of v4, /device:TPU:2, one launch (start us, length us, event | category | flops | bytes accessed | tf_op | source)
XLA Modules:
  0.0 151.3 jit_solution(17228579120252170375)
XLA Ops:
  0.0 149.8 %shard_map.73 = bf16[128,512]{1,0:T(8,128)(2,1)} custom-call(bf16[128,2048]{1,0:T(8,128)(2,1)} %tokens_ref.1, f32[1,2048]{1,0:T(1,128)} %bitcast.1, s32[8,256]{1,0:T(8,128)} %chosen_ref.1, f32[8,256]{1,0:T(8,128)} %weight_ref.1, bf16[8,256,1024]{2,1,0:T(8,128)(2,1)} %gate_hbm.1, bf16[8,256,1024]{2,1,0:T(8,128)(2,1)} %up_hbm.1, bf16[8,256,1024]{2,1,0:T(8,128)(2,1)} %down_hbm.1), custom_call_target="tpu_custom_call" | custom-call | tf_op jit(solution)/shard_map/pallas_call | solution.py:372
  149.8 1.6 %copy.9 = bf16[128,512]{1,0:T(8,128)(2,1)} copy(bf16[128,512]{1,0:T(8,128)(2,1)} %shard_map.73) | data formatting | bytes 262144
